TPU v7x, 32 devices: a whole 2x2x4 slice. The times are simulated.
32 devices in a mesh: sp: 8 (over z, x), tp: 4 (over y, core).
Axes of the slice: x: 2, y: 2, z: 4, core: 2. Of those that a mesh axis runs over, the one named last changes fastest.
Arguments:
- queries: bfloat16 [2048, 2048], P('sp', 'tp'), may hold values from -100 to 100
- key_columns: bfloat16 [1024, 2048], P('tp', 'sp'), may hold values from -24 to 24
- value_columns: bfloat16 [1024, 2048], P('tp', 'sp'), may hold values from -24 to 24
- sink_logits: float32 [32], P('tp'), may hold values from 3 to 7
- out_weight: bfloat16 [2048, 2048], P('tp'), may hold values from -0.1875 to 0.1875
- stream_in: bfloat16 [2048, 2048], P('sp'), may hold values from -3 to 3
- norm_gain: float32 [2048], replicated, may hold values from 0.1 to 1.9
- expert_ids: int32 [2048, 2], P('sp'), may hold values from 0 to 7, all different within a row; in each aligned block of 256 rows (0 to 255, 256 to 511, ...) at most 128 rows name the same one
- route_weights: float32 [2048, 2], P('sp'), may hold values from 0.1 to 0.7
- gate_weight: bfloat16 [8, 2048, 4096], P('sp', None, 'tp'), may hold values from -0.125 to 0.125
- up_weight: bfloat16 [8, 2048, 4096], P('sp', None, 'tp'), may hold values from -0.125 to 0.125
- down_weight: bfloat16 [8, 4096, 2048], P('sp', 'tp'), may hold values from -0.125 to 0.125
Outputs:
- layer_out: bfloat16 [2048, 2048], P('sp', 'tp')
Inputs may be any that keep to these rules, and one draw needn't show every extreme that they name: `expert_ids`: each row names 2 different experts. In each aligned block of 256 tokens no expert is named by more than 128 rows, and in some blocks one expert is named by exactly 128 rows.
All inputs are finite; a program needn't handle non-finite values.
Results may differ from a plain program's by a relative error of at most 0.02.
Values may be sent and summed in bfloat16 or wider, within the bound.
A program may use at most 64 MiB of HBM per device.

v0:
```python
import math

import jax
import jax.numpy as jnp
from jax import lax
from jax.sharding import PartitionSpec as P

HD = 64
WINDOW = 128


EPSILON = 1e-06
MASKED = -1e30


def padded(shard, sides, width):
    for axis, dim in sides:
        size, length = (lax.axis_size(axis), shard.shape[dim])
        up = [(i, (i + 1) % size) for i in range(size - 1)]
        down = [(j, i) for i, j in up]
        last = lax.slice_in_dim(shard, length - width, length, axis=dim)
        leading = lax.slice_in_dim(shard, 0, width, axis=dim)
        before = lax.ppermute(last, axis, up)
        after = lax.ppermute(leading, axis, down)
        shard = jnp.concatenate([before, shard, after], axis=dim)
    return shard


def rounded(number):
    return lax.optimization_barrier(number.astype(jnp.bfloat16)).astype(jnp.float32)


def rms_scale(residual, norm_gain):
    widened = residual.astype(jnp.float32)
    inverse_rms = lax.rsqrt(jnp.mean(widened * widened, axis=-1, keepdims=True) + EPSILON)
    return (widened * inverse_rms * norm_gain).astype(jnp.bfloat16)


def window_heads(queries, key_rims, value_rims, sink_logits, window, seq_start, seq_total):
    row_count = queries.shape[0]
    kv_heads = key_rims.shape[0] // HD
    q_heads = sink_logits.shape[0]
    per_group = q_heads // kv_heads
    blocks = row_count // window
    key_span = 3 * window
    query_blocks = queries.reshape(blocks, window, kv_heads, per_group, HD)
    starts = jnp.arange(blocks, dtype=jnp.int32) * window

    def take_span(source, offset):
        return lax.dynamic_slice_in_dim(source, offset, key_span, 1)

    key_blocks = jax.vmap(take_span, (None, 0))(key_rims, starts).reshape(
        blocks, kv_heads, HD, key_span
    )
    value_blocks = jax.vmap(take_span, (None, 0))(value_rims, starts).reshape(
        blocks, kv_heads, HD, key_span
    )
    scores = jnp.einsum(
        "bqkgd,bkdj->bkgqj", query_blocks, key_blocks, preferred_element_type=jnp.float32
    ) / math.sqrt(HD)
    query_pos = seq_start + starts[:, None] + jnp.arange(window, dtype=jnp.int32)[None, :]
    key_pos = seq_start + starts[:, None] - window + jnp.arange(key_span, dtype=jnp.int32)[None, :]
    visible = (
        (jnp.abs(query_pos[:, :, None] - key_pos[:, None, :]) <= window)
        & (key_pos[:, None, :] >= 0)
        & (key_pos[:, None, :] < seq_total)
    )
    visible = visible[:, None, None]
    scores = jnp.where(visible, scores, MASKED)
    sink_logit = sink_logits.reshape(kv_heads, per_group)[None, :, :, None]
    row_top = jnp.maximum(jnp.max(scores, axis=-1), sink_logit)
    exponent = jnp.where(visible, jnp.exp(scores - row_top[..., None]), 0.0)
    denominator = jnp.sum(exponent, axis=-1) + jnp.exp(sink_logit - row_top)
    attn_weights = (exponent / denominator[..., None]).astype(jnp.bfloat16)
    head_mix = jnp.einsum(
        "bkgqj,bkdj->bqkgd", attn_weights, value_blocks, preferred_element_type=jnp.float32
    )
    return head_mix.reshape(row_count, q_heads * HD).astype(jnp.bfloat16)


def route_slots(expert_ids, experts, capacity):
    flat_ids = expert_ids.reshape(-1)
    route_hits = (flat_ids[:, None] == jnp.arange(experts, dtype=jnp.int32)[None, :]).astype(
        jnp.int32
    )
    earlier = jnp.cumsum(route_hits, axis=0) - route_hits
    slot_index = jnp.sum(earlier * route_hits, axis=1)
    return flat_ids * capacity + slot_index


def expert_rows(arrived, gate_weight, up_weight, down_weight):
    sources, slot_count, feature_count = arrived.shape
    flat_rows = arrived.reshape(sources * slot_count, feature_count)
    gate_pre = jnp.dot(flat_rows, gate_weight[0], preferred_element_type=jnp.float32)
    upward = jnp.dot(flat_rows, up_weight[0], preferred_element_type=jnp.float32)
    hidden = (jax.nn.silu(gate_pre) * upward).astype(jnp.bfloat16)
    partial_out = jnp.dot(hidden, down_weight[0], preferred_element_type=jnp.float32)
    return partial_out.reshape(sources, slot_count, feature_count)


def send_back(partial_out):
    summed = lax.psum_scatter(
        partial_out.astype(jnp.bfloat16), "tp", scatter_dimension=2, tiled=True
    )
    return lax.all_to_all(summed, "sp", split_axis=0, concat_axis=0, tiled=True)


def local(
    queries,
    key_columns,
    value_columns,
    sink_logits,
    out_weight,
    stream_in,
    norm_gain,
    expert_ids,
    route_weights,
    gate_weight,
    up_weight,
    down_weight,
):
    tok_count = queries.shape[0]
    seq_devices = lax.axis_size("sp")
    tp_devices = lax.axis_size("tp")
    tp_index = lax.axis_index("tp")
    stacked = jnp.stack([key_columns, value_columns])
    with_rims = padded(stacked, (("sp", 2),), WINDOW)
    seq_start = lax.axis_index("sp") * tok_count
    head_out = window_heads(
        queries, with_rims[0], with_rims[1], sink_logits, WINDOW, seq_start, tok_count * seq_devices
    )
    col_count = stream_in.shape[1] // tp_devices
    partial_attn = jnp.dot(head_out, out_weight, preferred_element_type=jnp.float32)
    attn_sum = lax.psum(partial_attn.astype(jnp.bfloat16), "tp").astype(jnp.float32)
    residual = (stream_in.astype(jnp.float32) + rounded(attn_sum)).astype(jnp.bfloat16)
    normed = rms_scale(residual, norm_gain)
    residual_cols = lax.dynamic_slice_in_dim(residual, tp_index * col_count, col_count, 1)
    capacity = 4 * tok_count // seq_devices
    destination = route_slots(expert_ids, seq_devices, capacity)
    token_index = jnp.arange(destination.shape[0], dtype=jnp.int32) // expert_ids.shape[1]
    slot_token = (
        jnp.full((seq_devices * capacity,), tok_count, jnp.int32).at[destination].set(token_index)
    )
    outgoing = jnp.take(normed, slot_token, axis=0, mode="fill", fill_value=0)
    outgoing = outgoing.reshape(seq_devices, capacity, normed.shape[1])
    slot_share = capacity // tp_devices
    own_slots = lax.dynamic_slice_in_dim(outgoing, tp_index * slot_share, slot_share, 1)
    arrived = lax.all_to_all(own_slots, "sp", split_axis=0, concat_axis=0, tiled=True)
    partial_out = expert_rows(
        lax.all_gather(arrived, "tp", axis=1, tiled=True), gate_weight, up_weight, down_weight
    )
    returned = send_back(partial_out)
    picked = jnp.take(returned.reshape(seq_devices * capacity, col_count), destination, axis=0)
    picked = picked.reshape(tok_count, expert_ids.shape[1], col_count).astype(jnp.float32)
    expert_sum = jnp.sum(picked * route_weights[:, :, None], axis=1)
    return (residual_cols.astype(jnp.float32) + expert_sum).astype(jnp.bfloat16)


def solution(mesh):
    placed = (
        P("sp", "tp"),
        P("tp", "sp"),
        P("tp", "sp"),
        P("tp"),
        P("tp", None),
        P("sp", None),
        P(),
        P("sp", None),
        P("sp", None),
        P("sp", None, "tp"),
        P("sp", None, "tp"),
        P("sp", "tp", None),
    )
    return jax.shard_map(
        local, mesh=mesh, in_specs=placed, out_specs=P("sp", "tp"), check_vma=False
    )
```

profile of v0, /device:TPU:0, one launch (start us, length us, event | category | flops | bytes accessed | tf_op | source)
XLA Modules:
  0.0 264.0 jit_solution(4247613377769468337)
XLA Ops:
  6.5 1.1 fusion.25
  7.6 4.9 %collective-permute-start = (bf16[2,256,128]{2,1,0:T(8,128)(2,1)S(1)}, bf16[2,256,128]{2,1,0:T(8,128)(2,1)S(1)}, u32[]{:S(2)}, u32[]{:S(2)}) collective-permute-start(bf16[2,256,128]{2,1,0:T(8,128)(2,1)S(1)} %get-tuple-element.41), channel_id=1, source_target_pairs={{0,4},{4,8},{8,12},{12,16},{16,20},{20,24},{24,28},{1,5},{5,9},{9,... | collective-permute-start | bytes 393224 | tf_op jit(solution)/shard_map/ppermute | solution.py:23
  12.5 1.3 collective-permute-start.1
  13.8 0.1 fusion.36
  13.9 0.1 iota_add_fusion
  14.0 0.8 copy.29
  14.8 0.1 eq.26
  15.0 0.1 reshape.217
  15.1 0.7 broadcast_multiply_fusion
  15.9 0.7 concatenate.8
  16.5 1.3 reshape.287
  17.8 0.7 max.17
  18.5 1.1 reduce-window.6
  19.7 0.2 slice_reduce_fusion
  19.9 0.1 copy.33
  20.1 0.1 mul.90
  20.2 0.1 fusion.27
  20.3 2.4 scatter_custom_fusion
  22.8 1.1 fusion.22
  23.9 1.0 pad_maximum_fusion
  25.0 4.3 %while.3 = (s32[]{:T(128)}, bf16[256,512]{1,0:T(8,128)(2,1)S(1)}, s32[2,2]{1,0:T(2,128)}, bf16[2,256,384]{2,1,0:T(8,128)(2,1)S(1)}, s32[]{:T(128)}) while((s32[]{:T(128)}, bf16[256,512]{1,0:T(8,128)(2,1)S(1)}, s32[2,2]{1,0:T(2,128)}, bf16[2,256,384]{2,1,0:T(8,128)(2,1)S(1)}, s32[]{:T(128)}) %tuple.36), condition=%wide.while_cond.1, body=%wide.while_body.1.sunk | while | flops 2 | bytes 393313 | solution.py:50
  25.0 0.7 constant_dynamic-slice_fusion.6
  25.7 0.6 slice.67
  26.4 0.8 bitcast_dynamic-update-slice_fusion.5
  27.2 0.7 constant_dynamic-slice_fusion.6
  27.9 0.6 slice.67
  28.5 0.8 bitcast_dynamic-update-slice_fusion.5
  29.3 1.7 fusion.9
  31.0 0.1 broadcast_maximum_fusion
  31.0 1.6 copy-done.1
  32.6 0.8 fusion.12
  33.4 0.1 exponential_add_fusion
  33.5 2.8 %while.2 = (s32[]{:T(128)}, bf16[256,512]{1,0:T(8,128)(2,1)S(1)}, s32[2,2]{1,0:T(2,128)S(1)}, bf16[2,256,384]{2,1,0:T(8,128)(2,1)S(1)}, s32[]{:T(128)}) while((s32[]{:T(128)}, bf16[256,512]{1,0:T(8,128)(2,1)S(1)}, s32[2,2]{1,0:T(2,128)S(1)}, bf16[2,256,384]{2,1,0:T(8,128)(2,1)S(1)}, s32[]{:T(128)}) %tuple.45), condition=%wide.while_cond, body=%wide.while_body.sunk | while | flops 2 | bytes 393313 | solution.py:50
  33.5 0.6 slice.66
  34.1 0.8 bitcast_dynamic-update-slice_fusion.4
  34.9 0.6 slice.66
  35.5 0.8 bitcast_dynamic-update-slice_fusion.4
  36.3 2.9 %fusion.18 = bf16[2,128,4,2,64]{1,4,3,2,0:T(8,128)(2,1)S(1)} fusion(bf16[2,4,64,384,1]{3,2,4,1,0:T(8,128)(2,1)S(1)} %bitcast.98, f32[2,4,384,128,2]{3,2,4,1,0:T(8,128)} %copy-done.1, f32[2,4,2,128]{3,2,1,0:T(2,128)S(1)} %exponential_add_fusion, f32[2,4,2,128]{3,2,1,0:T(2,128)S(1)} %broadcast_maximum_fusion, pred[2,128,384]{1,2,0:T(8,128)(4,1)S(1)} %copy-done.4), kind=kOutput, calls=%fused_computation.29 | convolution fusion | flops 105512960 | bytes 3915776 | tf_op jit(solution)/shard_map/bkgqj,bkdj->bqkgd/dot_general | solution.py:75
  39.3 0.3 copy.28
  39.6 1.8 convolution_convert_fusion
  41.4 0.1 constant_dynamic-slice_fusion.2
  41.5 38.7 %all-reduce.3.cloned.1.call-done = bf16[256,2048]{1,0:T(8,128)(2,1)} async-done(((bf16[256,2048]{1,0:T(8,128)(2,1)}), bf16[256,2048]{1,0:T(8,128)(2,1)}) %all-reduce.3.cloned.1.call-update) | async-done | bytes 1048592 | tf_op jit(solution)/shard_map/psum | solution.py:134
  80.2 1.7 fusion.13
  81.9 0.9 copy-done.2
  82.9 0.3 fusion.15
  83.2 6.0 %gather_fusion = bf16[1024,2048]{1,0:T(8,128)(2,1)} fusion(bf16[256,2048]{1,0:T(8,128)(2,1)S(1)} %fusion.15, s32[1024]{0:T(1024)S(1)} %fusion.29), kind=kCustom, calls=%fused_computation | custom fusion | bytes 8392704 | tf_op jit(solution)/shard_map/jit(_take)/gather | solution.py:144
  89.2 1.5 dynamic-slice_select_fusion
  90.7 30.6 %all_to_all.10 = bf16[8,32,2048]{2,1,0:T(8,128)(2,1)} all-to-all(bf16[8,32,2048]{2,1,0:T(8,128)(2,1)S(1)} %dynamic-slice_select_fusion), channel_id=1, replica_groups=mesh['sp'=8,'tp'=4] {'sp'}, dimensions={0} | all-to-all | bytes 2097152 | tf_op jit(solution)/shard_map/all_to_all | solution.py:148
  121.3 0.2 reduce-scatter.2.cloned.1.call-start
  121.6 33.3 %all-gather.2.cloned.1.call-done = bf16[8,128,2048]{2,1,0:T(8,128)(2,1)} async-done(((bf16[8,32,2048]{2,1,0:T(8,128)(2,1)}), bf16[8,128,2048]{2,1,0:T(8,128)(2,1)}) %all-gather.2.cloned.1.call-update) | async-done | bytes 4194320 | tf_op jit(solution)/shard_map/all_gather | solution.py:150
  154.8 7.7 %fusion.2 = f32[1024,1024]{1,0:T(8,128)S(1)} fusion(bf16[1024,2048]{1,0:T(8,128)(2,1)} %bitcast.102, bf16[1,2048,1024]{2,1,0:T(8,128)(2,1)} %param.22), kind=kOutput, calls=%fused_computation.9 | convolution fusion | flops 4294967296 | bytes 12582912 | tf_op jit(solution)/shard_map/dot_general | solution.py:95
  162.5 5.4 %multiply_convert_fusion = bf16[1024,1024]{1,0:T(8,128)(2,1)S(1)} fusion(f32[1024,1024]{1,0:T(8,128)S(1)} %fusion.2, bf16[1024,2048]{1,0:T(8,128)(2,1)S(1)} %bitcast.103, bf16[1,2048,1024]{2,1,0:T(8,128)(2,1)S(1)} %copy-done.9), kind=kOutput, calls=%fused_computation.13 | convolution fusion | flops 4301258752 | bytes 14680064 | tf_op jit(solution)/shard_map/dot_general | solution.py:94
  167.9 6.1 %fusion.6 = bf16[8,128,2048]{2,1,0:T(8,128)(2,1)} fusion(bf16[8,128,1024]{2,1,0:T(8,128)(2,1)S(1)} %bitcast.104, bf16[1,1024,2048]{2,1,0:T(8,128)(2,1)S(1)} %copy-done.10), kind=kOutput, calls=%fused_computation.14 | convolution fusion | flops 4297064448 | bytes 10485760 | tf_op jit(solution)/shard_map/dot_general | solution.py:97
  174.0 44.5 %reduce-scatter.2.cloned.1.call-done = bf16[8,128,512]{2,1,0:T(8,128)(2,1)} async-done(((bf16[8,128,2048]{2,1,0:T(8,128)(2,1)}), bf16[8,128,512]{2,1,0:T(8,128)(2,1)}) %reduce-scatter.2.cloned.1.call-update) | async-done | bytes 1048592 | tf_op jit(solution)/shard_map/reduce_scatter | solution.py:102
  218.5 5.5 %all-to-all-start.1 = ((bf16[8,128,512]{2,1,0:T(8,128)(2,1)}), bf16[8,128,512]{2,1,0:T(8,128)(2,1)S(1)}, u32[]{:S(2)}, u32[]{:S(2)}) async-start(bf16[8,128,512]{2,1,0:T(8,128)(2,1)} %reduce-scatter.2.cloned.1.call-done), calls=%async_computation.2 | async-start | bytes 2097152 | tf_op jit(solution)/shard_map/all_to_all | solution.py:105
  224.1 0.1 reduce_sum.42
  224.2 0.1 copy.31
  224.3 0.2 copy.32
  224.5 0.1 copy.34
  224.7 25.1 %all-to-all-done.1 = bf16[8,128,512]{2,1,0:T(8,128)(2,1)S(1)} async-done(((bf16[8,128,512]{2,1,0:T(8,128)(2,1)}), bf16[8,128,512]{2,1,0:T(8,128)(2,1)S(1)}, u32[]{:S(2)}, u32[]{:S(2)}) %all-to-all-start.1) | async-done | bytes 1048608 | tf_op jit(solution)/shard_map/all_to_all | solution.py:105
  249.7 2.6 gather_fusion.1
  252.3 1.2 gather.23
  253.6 2.2 multiply_reduce_fusion
  255.8 1.7 add_convert_fusion.1
  (47 shorter events, 0.5 us)
Async XLA Ops:
  6.5 33.0 %copy-start = (bf16[512,2048]{1,0:T(8,128)(2,1)S(1)}, bf16[512,2048]{1,0:T(8,128)(2,1)}, u32[]{:S(2)}) copy-start(bf16[512,2048]{1,0:T(8,128)(2,1)} %param.16) | copy-start | bytes 6291460
  6.5 73.7 %all-reduce.3.cloned.1.call-start = ((), (), s32[]{:S(2)}) async-start(), calls=%async_computation.3 | async-start | bytes 2097152 | tf_op jit(solution)/shard_map/psum | solution.py:134
  7.6 16.3 %collective-permute-start = (bf16[2,256,128]{2,1,0:T(8,128)(2,1)S(1)}, bf16[2,256,128]{2,1,0:T(8,128)(2,1)S(1)}, u32[]{:S(2)}, u32[]{:S(2)}) collective-permute-start(bf16[2,256,128]{2,1,0:T(8,128)(2,1)S(1)} %get-tuple-element.41), channel_id=1, source_target_pairs={{0,4},{4,8},{8,12},{12,16},{16,20},{20,24},{24,28},{1,5},{5,9},{9,... | collective-permute-start | bytes 393224 | tf_op jit(solution)/shard_map/ppermute | solution.py:23
  12.5 11.4 %collective-permute-start.1 = (bf16[2,256,128]{2,1,0:T(8,128)(2,1)S(1)}, bf16[2,256,128]{2,1,0:T(8,128)(2,1)S(1)}, u32[]{:S(2)}, u32[]{:S(2)}) collective-permute-start(bf16[2,256,128]{2,1,0:T(8,128)(2,1)S(1)} %get-tuple-element.42), channel_id=1, source_target_pairs={{4,0},{8,4},{12,8},{16,12},{20,16},{24,20},{28,24},{5,1},{9,5},{13... | collective-permute-start | bytes 393224 | tf_op jit(solution)/shard_map/ppermute | solution.py:24
  29.3 3.3 %copy-start.4 = (pred[2,128,384]{1,2,0:T(8,128)(4,1)S(1)}, pred[2,128,384]{1,2,0:T(8,128)(4,1)}, u32[]{:S(2)}) copy-start(pred[2,128,384]{1,2,0:T(8,128)(4,1)} %fusion.22) | copy-start | bytes 294916
  31.0 1.7 copy-start.1
  31.0 2.5 copy-start.8
  39.3 40.9 %copy-start.3 = (bf16[256,2048]{1,0:T(8,128)(2,1)S(1)}, bf16[256,2048]{1,0:T(8,128)(2,1)}, u32[]{:S(2)}) copy-start(bf16[256,2048]{1,0:T(8,128)(2,1)} %param.17) | copy-start | bytes 3145732
  39.6 43.3 %copy-start.6 = (f32[2048]{0:T(1024)S(1)}, f32[2048]{0:T(1024)}, u32[]{:S(2)}) copy-start(f32[2048]{0:T(1024)} %param.18) | copy-start | bytes 24580
  41.4 113.5 %all-gather.2.cloned.1.call-start = ((), (), s32[]{:S(2)}) async-start(), calls=%async_computation.4 | async-start | bytes 5242880 | tf_op jit(solution)/shard_map/all_gather | solution.py:150
  81.9 1.0 copy-start.2
  121.3 97.2 %reduce-scatter.2.cloned.1.call-start = ((), (), s32[]{:S(2)}) async-start(), calls=%async_computation.5 | async-start | bytes 5242880 | tf_op jit(solution)/shard_map/reduce_scatter | solution.py:102
  154.8 7.7 %copy-start.9 = (bf16[1,2048,1024]{2,1,0:T(8,128)(2,1)S(1)}, bf16[1,2048,1024]{2,1,0:T(8,128)(2,1)}, u32[]{:S(2)}) copy-start(bf16[1,2048,1024]{2,1,0:T(8,128)(2,1)} %param.21) | copy-start | bytes 12582916
  154.8 7.7 %copy-start.11 = (bf16[8,128,2048]{2,1,0:T(8,128)(2,1)S(1)}, bf16[8,128,2048]{2,1,0:T(8,128)(2,1)}, u32[]{:S(2)}) copy-start(bf16[8,128,2048]{2,1,0:T(8,128)(2,1)} %all-gather.2.cloned.1.call-done) | copy-start | bytes 12582916
  162.5 5.4 %copy-start.10 = (bf16[1,1024,2048]{2,1,0:T(8,128)(2,1)S(1)}, bf16[1,1024,2048]{2,1,0:T(8,128)(2,1)}, u32[]{:S(2)}) copy-start(bf16[1,1024,2048]{2,1,0:T(8,128)(2,1)} %param.23) | copy-start | bytes 12582916
  174.0 50.3 %copy-start.5 = (s32[256,2]{0,1:T(2,128)S(1)}, s32[256,2]{0,1:T(2,128)}, u32[]{:S(2)}) copy-start(s32[256,2]{0,1:T(2,128)} %param.19) | copy-start | bytes 6148
  174.0 50.5 %copy-start.7 = (f32[256,2]{0,1:T(2,128)S(1)}, f32[256,2]{0,1:T(2,128)}, u32[]{:S(2)}) copy-start(f32[256,2]{0,1:T(2,128)} %param.20) | copy-start | bytes 6148
  218.5 31.2 %all-to-all-start.1 = ((bf16[8,128,512]{2,1,0:T(8,128)(2,1)}), bf16[8,128,512]{2,1,0:T(8,128)(2,1)S(1)}, u32[]{:S(2)}, u32[]{:S(2)}) async-start(bf16[8,128,512]{2,1,0:T(8,128)(2,1)} %reduce-scatter.2.cloned.1.call-done), calls=%async_computation.2 | async-start | bytes 2097152 | tf_op jit(solution)/shard_map/all_to_all | solution.py:105
Sparse Core Ops, SparseCore 0:
  41.5 38.6 all-reduce.2
  121.5 33.3 all-gather.1
  174.1 44.3 reduce-scatter.1
where the time goes:
time: 265 us; the launch traced here: 264 us
  waiting for transfers between devices  142 us (54%)
  blocking collectives  30.6 us (12%)
  local copies, waits for them, and re-layouts  27 us (10%)
  matrix products  25.4 us (10%)
  other arithmetic  13.8 us (5%)
  between operations  13.5 us (5%)
  starting transfers between devices  12 us (5%)
    reduce_scatter x1, waiting for transfers between devices, send_back(): lax.psum_scatter(partial_out.astype(jnp.bfloat16), 'tp', scatter_dimensio...  44.5 us
    psum x1, waiting for transfers between devices, local(): lax.psum(partial_attn.astype(jnp.bfloat16), 'tp').astype(jnp.float32)  38.7 us
    all_gather x1, waiting for transfers between devices, local(): lax.all_gather(arrived, 'tp', axis=1, tiled=True)  33.3 us
    all_to_all x1, blocking collectives, local(): lax.all_to_all(own_slots, 'sp', split_axis=0, concat_axis=0, tiled=True)  30.6 us
    all_to_all x1, waiting for transfers between devices, send_back(): return lax.all_to_all(summed, 'sp', split_axis=0, concat_axis=0, tiled=True)  25.1 us
    dot_general x1, matrix products, expert_rows(): jnp.dot(flat_rows, up_weight[0], preferred_element_type=jnp.float32)  7.65 us
    gather x12, local copies, waits for them, and re-layouts  6.95 us
    dot_general x1, matrix products, expert_rows(): jnp.dot(hidden, down_weight[0], preferred_element_type=jnp.float32)  6.07 us
  transfers between devices with their start and end apart: 6, of which 4 were waited for; matrix products, arithmetic and copies ran while one was open for 4% of the time, Pallas kernels for 0%

commit v1 on v0

v1 whole, which is shorter than its diff:
```python
import functools
import math

import jax
import jax.numpy as jnp
from jax import lax
from jax.experimental import pallas as pl
from jax.experimental.pallas import tpu as pltpu
from jax.sharding import PartitionSpec as P

HD = 64
WINDOW = 128
CORES = 2
EPSILON = 1e-06
MASKED = -1e30
MESH = pl.DeviceIdType.MESH
F32 = jnp.float32
BF16 = jnp.bfloat16


def iota(shape, dim):
    return lax.broadcasted_iota(jnp.int32, shape, dim)


def dot(a, b):
    return jnp.dot(a, b, preferred_element_type=F32)


def as_row(column):
    size = column.shape[0]
    eye = iota((size, size), 0) == iota((size, size), 1)
    return jnp.sum(jnp.where(eye, column, 0.0), axis=0, keepdims=True)


def as_column(row):
    size = row.shape[1]
    eye = iota((size, size), 0) == iota((size, size), 1)
    return jnp.sum(jnp.where(eye, row, 0.0), axis=1, keepdims=True)


def send(src, dst, send_sem, recv_sem, device):
    copy = pltpu.make_async_remote_copy(
        src_ref=src,
        dst_ref=dst,
        send_sem=send_sem,
        recv_sem=recv_sem,
        device_id=device,
        device_id_type=MESH,
    )
    copy.start()


def sent(ref, sem, device):
    pltpu.make_async_remote_copy(
        src_ref=ref, dst_ref=ref, send_sem=sem, recv_sem=sem,
        device_id=device, device_id_type=MESH,
    ).wait_send()


def landed(ref, sem, device):
    pltpu.make_async_remote_copy(
        src_ref=ref, dst_ref=ref, send_sem=sem, recv_sem=sem,
        device_id=device, device_id_type=MESH,
    ).wait_recv()


def layer(
    n, tp, cap,
    q_ref, k_ref, v_ref, sink_ref, gain_ref, ids_ref, rw_ref,
    ow_hbm, stream_hbm, gate_hbm, up_hbm, down_hbm,
    out_ref,
    ow, stream, gate, up, down,
    halo, head, part, part_in, part_sum, part_y, squares,
    slots, xb, hid, po, po_in, chip_sum, sum_y, final, back, residual,
    load_sem, halo_send, halo_recv, ps_send, ps_recv, py_send, py_recv, sq_send, sq_recv,
    d_send, x_recv, fc_send, fy_send, f2_send,
    po_send, po_recv, y_send, y_recv, r_send, r_recv,
):
    s, t = lax.axis_index("sp"), lax.axis_index("tp")
    ny = tp // CORES
    y, c = t // CORES, lax.rem(t, CORES)
    other = 1 - c
    tok, width = residual.shape
    hidden = gate.shape[1]

    def at_sp(i):
        return (i, t)

    def at_tp(j):
        return (s, j)

    partner = at_tp(y * CORES + other)

    def peer_y(dy):
        return lax.rem(y + dy, ny)

    def from_y(dy):
        return lax.rem(y + ny - dy, ny)

    loads = [
        pltpu.make_async_copy(ow_hbm, ow, load_sem.at[0]),
        pltpu.make_async_copy(
            stream_hbm.at[:, pl.ds(pl.multiple_of(t * width, 128), width)], stream, load_sem.at[1]
        ),
        pltpu.make_async_copy(gate_hbm.at[0], gate, load_sem.at[2]),
        pltpu.make_async_copy(up_hbm.at[0], up, load_sem.at[3]),
        pltpu.make_async_copy(down_hbm.at[0], down, load_sem.at[4]),
    ]
    for load in loads:
        load.start()

    barrier = pltpu.get_barrier_semaphore()

    def greet_sp(i, _):
        pl.semaphore_signal(
            barrier, inc=1, device_id=at_sp(lax.rem(s + i, n)), device_id_type=MESH
        )
        return 0

    def greet_tp(j, _):
        pl.semaphore_signal(
            barrier, inc=1, device_id=at_tp(lax.rem(t + j, tp)), device_id_type=MESH
        )
        return 0

    lax.fori_loop(1, n, greet_sp, 0)
    lax.fori_loop(1, tp, greet_tp, 0)
    pl.semaphore_wait(barrier, n - 1 + tp - 1)

    right, left = at_sp(lax.rem(s + 1, n)), at_sp(lax.rem(s + n - 1, n))
    for a, source in enumerate((k_ref, v_ref)):
        send(source.at[:, pl.ds(tok - WINDOW, WINDOW)], halo.at[a, 0],
             halo_send.at[a, 0], halo_recv.at[a, 0], right)
        send(source.at[:, pl.ds(0, WINDOW)], halo.at[a, 1],
             halo_send.at[a, 1], halo_recv.at[a, 1], left)

    experts = n
    ids = ids_ref[...]
    lanes = iota((tok, 128), 1)
    top = ids.shape[1]
    hits = [(lanes == ids[:, k : k + 1]).astype(F32) for k in range(top)]
    all_hits = functools.reduce(jnp.add, hits)
    before = (iota((tok, tok), 1) < iota((tok, tok), 0)).astype(BF16)
    earlier = dot(before, all_hits.astype(BF16))
    place = [
        jnp.sum(earlier * hits[k], axis=1, keepdims=True) + ids[:, k : k + 1].astype(F32) * cap
        for k in range(top)
    ]
    place_row = [as_row(p) for p in place]

    for a, source in enumerate((k_ref, v_ref)):
        landed(halo.at[a, 0], halo_recv.at[a, 0], left)
        landed(halo.at[a, 1], halo_recv.at[a, 1], right)

    kv_heads = k_ref.shape[0] // HD
    group = q_ref.shape[1] // HD // kv_heads
    span = 3 * WINDOW
    row = lax.rem(iota((group * WINDOW, span), 0), WINDOW)
    col = iota((group * WINDOW, span), 1)
    near = (col - row >= 0) & (col - row <= 2 * WINDOW)
    for b in range(tok // WINDOW):
        key_pos = s * tok + (b - 1) * WINDOW + col
        visible = near & (key_pos >= 0) & (key_pos < n * tok)
        rows = pl.ds(b * WINDOW, WINDOW)
        for g in range(kv_heads):
            feats = pl.ds(g * HD, HD)
            kx, vx = [
                jnp.concatenate(
                    [halo[a, 0, feats, :], ref[feats, :], halo[a, 1, feats, :]], axis=1
                )[:, b * WINDOW : b * WINDOW + span]
                for a, ref in enumerate((k_ref, v_ref))
            ]
            qs = jnp.concatenate(
                [q_ref[rows, pl.ds((g * group + h) * HD, HD)] for h in range(group)], axis=0
            )
            sink = jnp.concatenate(
                [jnp.full((WINDOW, 1), sink_ref[g * group + h], F32) for h in range(group)], axis=0
            )
            scores = jnp.where(visible, dot(qs, kx) * (1.0 / math.sqrt(HD)), MASKED)
            row_top = jnp.maximum(jnp.max(scores, axis=1, keepdims=True), sink)
            weight = jnp.where(visible, jnp.exp(scores - row_top), 0.0)
            total = jnp.sum(weight, axis=1, keepdims=True) + jnp.exp(sink - row_top)
            weight = (weight * (1.0 / total)).astype(BF16)
            mixed = lax.dot_general(
                weight, vx, (((1,), (1,)), ((), ())), preferred_element_type=F32
            ).astype(BF16)
            head[rows, pl.ds(g * group * HD, group * HD)] = jnp.concatenate(
                [mixed[h * WINDOW : (h + 1) * WINDOW] for h in range(group)], axis=1
            )

    loads[0].wait()
    loads[1].wait()

    def project(core):
        for yy in range(ny):
            start = pl.multiple_of((yy * CORES + core) * width, 128)
            part[core, yy] = dot(head[...], ow[:, pl.ds(start, width)]).astype(BF16)

    project(other)
    send(part.at[other], part_in, ps_send, ps_recv, partner)
    project(c)
    landed(part_in, ps_recv, partner)
    for dy in range(1, ny):
        yy = peer_y(dy)
        part_sum[dy] = (part[c, yy].astype(F32) + part_in[yy].astype(F32)).astype(BF16)
        send(part_sum.at[dy], part_y.at[dy], py_send.at[dy], py_recv.at[dy],
             at_tp(yy * CORES + c))
    attn = part[c, y].astype(F32) + part_in[y].astype(F32)
    for dy in range(1, ny):
        landed(part_y.at[dy], py_recv.at[dy], at_tp(from_y(dy) * CORES + c))
        attn = attn + part_y[dy].astype(F32)
    res = (stream[...].astype(F32) + attn.astype(BF16).astype(F32)).astype(BF16)
    residual[...] = res
    res = res.astype(F32)
    own_squares = jnp.broadcast_to(as_row(jnp.sum(res * res, axis=1, keepdims=True)), (8, tok))
    squares[0] = own_squares
    for dt in range(1, tp):
        send(squares.at[0], squares.at[dt], sq_send.at[dt], sq_recv.at[dt],
             at_tp(lax.rem(t + dt, tp)))
    square_sum = own_squares
    for dt in range(1, tp):
        landed(squares.at[dt], sq_recv.at[dt], at_tp(lax.rem(t + tp - dt, tp)))
        square_sum = square_sum + squares[dt]
    inverse = as_column(lax.rsqrt(square_sum[0:1] / (tp * width) + EPSILON))
    gain = gain_ref[:, pl.ds(pl.multiple_of(t * width, 128), width)]
    normed = (res * inverse * gain).astype(BF16)

    slot = iota((cap, tok), 0)

    def rows_of(e):
        wanted = (slot + e * cap).astype(F32)
        pick = functools.reduce(jnp.logical_or, [wanted == p for p in place_row])
        return dot(pick.astype(F32).astype(BF16), normed).astype(BF16)

    xb[t, s] = rows_of(s)

    def dispatch(i, _):
        e = lax.rem(s + i, n)
        slots[i] = rows_of(e)
        send(slots.at[i], xb.at[t, s], d_send.at[i], x_recv.at[t, s], at_sp(e))
        return 0

    lax.fori_loop(1, n, dispatch, 0)
    for load in loads[2:]:
        load.wait()

    def forward(i):
        src = lax.rem(s + n - i, n)

        @pl.when(i > 0)
        def _():
            landed(xb.at[t, src], x_recv.at[t, src], at_sp(src))

        for dy in range(1, ny):
            send(xb.at[t, src], xb.at[t, src], fy_send.at[dy, i], x_recv.at[t, src],
                 at_tp(peer_y(dy) * CORES + c))
        send(xb.at[t, src], xb.at[t, src], fc_send.at[i], x_recv.at[t, src], partner)

    def relay(i):
        src = lax.rem(s + n - i, n)
        for dy in range(1, ny):
            j = from_y(dy) * CORES + c
            landed(xb.at[j, src], x_recv.at[j, src], at_tp(j))
            send(xb.at[j, src], xb.at[j, src], f2_send.at[dy, i], x_recv.at[j, src], partner)

    tile = min(hidden, 256)

    def expert(i):
        src = lax.rem(s + n - i, n)
        for yy in range(ny):
            j = yy * CORES + other
            landed(xb.at[j, src], x_recv.at[j, src], partner)
        rows = jnp.concatenate([xb[j, src] for j in range(tp)], axis=1)
        for f in range(hidden // tile):
            cols = pl.ds(f * tile, tile)
            gate_pre = dot(rows, gate[:, cols])
            upward = dot(rows, up[:, cols])
            hid[:, cols] = (gate_pre / (1.0 + jnp.exp(-gate_pre)) * upward).astype(BF16)
        for j in range(tp):
            po[i, j % CORES, j // CORES] = dot(
                hid[...], down[:, j * width : (j + 1) * width]
            ).astype(BF16)
        send(po.at[i, other], po_in.at[i], po_send.at[i], po_recv.at[i], partner)

    def chip_add(i):
        landed(po_in.at[i], po_recv.at[i], partner)
        for dy in range(1, ny):
            yy = peer_y(dy)
            chip_sum[dy, i] = (po[i, c, yy].astype(F32) + po_in[i, yy].astype(F32)).astype(BF16)
            send(chip_sum.at[dy, i], sum_y.at[dy, i], y_send.at[dy, i], y_recv.at[dy, i],
                 at_tp(yy * CORES + c))

    def finish(i):
        src = lax.rem(s + n - i, n)
        total = po[i, c, y].astype(F32) + po_in[i, y].astype(F32)
        for dy in range(1, ny):
            landed(sum_y.at[dy, i], y_recv.at[dy, i], at_tp(from_y(dy) * CORES + c))
            total = total + sum_y[dy, i].astype(F32)

        @pl.when(i == 0)
        def _():
            back[s] = total.astype(BF16)

        @pl.when(i > 0)
        def _():
            final[i] = total.astype(BF16)
            send(final.at[i], back.at[s], r_send.at[i], r_recv.at[s], at_sp(src))

    stages = (forward, relay, expert, chip_add, finish)

    def step(k, _):
        for lag, stage in enumerate(stages):
            @pl.when((k >= lag) & (k - lag < n))
            def _(stage=stage, lag=lag):
                stage(k - lag)
        return 0

    lax.fori_loop(0, n + len(stages) - 1, step, 0)

    def returned(i, _):
        e = lax.rem(s + i, n)
        landed(back.at[e], r_recv.at[e], at_sp(e))
        return 0

    lax.fori_loop(1, n, returned, 0)

    rows = back[...].reshape(n * cap, width)
    spot = iota((tok, n * cap), 1).astype(F32)
    mixture = jnp.zeros((tok, width), F32)
    for k in range(top):
        pick = (spot == place[k]).astype(F32).astype(BF16)
        mixture = mixture + rw_ref[:, k : k + 1] * dot(pick, rows)
    out_ref[...] = (residual[...].astype(F32) + mixture).astype(BF16)

    for a, source in enumerate((k_ref, v_ref)):
        sent(halo.at[a, 0], halo_send.at[a, 0], right)
        sent(halo.at[a, 1], halo_send.at[a, 1], left)
    sent(part.at[other], ps_send, partner)
    for dy in range(1, ny):
        sent(part_sum.at[dy], py_send.at[dy], partner)
    for dt in range(1, tp):
        sent(squares.at[0], sq_send.at[dt], partner)

    def drain(i, _):
        @pl.when(i > 0)
        def _():
            sent(slots.at[i], d_send.at[i], right)
            sent(final.at[i], r_send.at[i], right)

        sent(final.at[i], fc_send.at[i], partner)
        sent(po_in.at[i], po_send.at[i], partner)
        for dy in range(1, ny):
            sent(final.at[i], fy_send.at[dy, i], partner)
            sent(final.at[i], f2_send.at[dy, i], partner)
            sent(final.at[i], y_send.at[dy, i], partner)
        return 0

    lax.fori_loop(0, n, drain, 0)


def local(
    n, tp,
    queries, key_columns, value_columns, sink_logits, out_weight, stream_in, norm_gain,
    expert_ids, route_weights, gate_weight, up_weight, down_weight,
):
    tok, features = stream_in.shape
    ny = tp // CORES
    cap = 4 * tok // n
    width = features // tp
    hidden = gate_weight.shape[2]
    kv = key_columns.shape[0]
    dma = pltpu.SemaphoreType.DMA
    vmem = pl.BlockSpec(memory_space=pltpu.VMEM)
    hbm = pl.BlockSpec(memory_space=pl.ANY)
    smem = pl.BlockSpec(memory_space=pltpu.SMEM)
    scratch = [
        pltpu.VMEM(out_weight.shape, BF16),
        pltpu.VMEM((tok, width), BF16),
        pltpu.VMEM(gate_weight.shape[1:], BF16),
        pltpu.VMEM(up_weight.shape[1:], BF16),
        pltpu.VMEM(down_weight.shape[1:], BF16),
        pltpu.VMEM((2, 2, kv, WINDOW), BF16),
        pltpu.VMEM(queries.shape, BF16),
        pltpu.VMEM((CORES, ny, tok, width), BF16),
        pltpu.VMEM((ny, tok, width), BF16),
        pltpu.VMEM((ny, tok, width), BF16),
        pltpu.VMEM((ny, tok, width), BF16),
        pltpu.VMEM((tp, 8, tok), F32),
        pltpu.VMEM((n, cap, width), BF16),
        pltpu.VMEM((tp, n, cap, width), BF16),
        pltpu.VMEM((cap, hidden), BF16),
        pltpu.VMEM((n, CORES, ny, cap, width), BF16),
        pltpu.VMEM((n, ny, cap, width), BF16),
        pltpu.VMEM((ny, n, cap, width), BF16),
        pltpu.VMEM((ny, n, cap, width), BF16),
        pltpu.VMEM((n, cap, width), BF16),
        pltpu.VMEM((n, cap, width), BF16),
        pltpu.VMEM((tok, width), BF16),
        dma((5,)),
        dma((2, 2)), dma((2, 2)),
        dma, dma,
        dma((ny,)), dma((ny,)),
        dma((tp,)), dma((tp,)),
        dma((n,)), dma((tp, n)), dma((n,)), dma((ny, n)), dma((ny, n)),
        dma((n,)), dma((n,)),
        dma((ny, n)), dma((ny, n)),
        dma((n,)), dma((n,)),
    ]
    return pl.pallas_call(
        functools.partial(layer, n, tp, cap),
        out_shape=jax.ShapeDtypeStruct((tok, width), BF16),
        in_specs=[vmem, vmem, vmem, smem, vmem, vmem, vmem] + [hbm] * 5,
        out_specs=vmem,
        scratch_shapes=scratch,
        compiler_params=pltpu.CompilerParams(
            collective_id=0, has_side_effects=True, vmem_limit_bytes=60 * 1024 * 1024
        ),
    )(
        queries, key_columns, value_columns, sink_logits, norm_gain[None, :], expert_ids,
        route_weights, out_weight, stream_in, gate_weight, up_weight, down_weight,
    )


def solution(mesh):
    placed = (
        P("sp", "tp"),
        P("tp", "sp"),
        P("tp", "sp"),
        P("tp"),
        P("tp", None),
        P("sp", None),
        P(),
        P("sp", None),
        P("sp", None),
        P("sp", None, "tp"),
        P("sp", None, "tp"),
        P("sp", "tp", None),
    )
    return jax.shard_map(
        functools.partial(local, mesh.shape["sp"], mesh.shape["tp"]),
        mesh=mesh, in_specs=placed, out_specs=P("sp", "tp"), check_vma=False,
    )
```

time: 265 us -> 105 us (0.40)
  waiting for transfers between devices: 142 us -> 0 us
  Pallas kernels: 0 us -> 100 us
  blocking collectives: 30.6 us -> 0 us
  matrix products: 25.4 us -> 0 us
  local copies, waits for them, and re-layouts: 27 us -> 4.62 us
  other arithmetic: 13.8 us -> 0 us
  between operations: 13.5 us -> 0.01 us
  starting transfers between devices: 12 us -> 0 us
    pallas_call x0 -> x1, Pallas kernels: none -> 100 us  [local(): pl.pallas_call(functools.partial(layer, n, tp, cap), out_shape=jax.ShapeD...]
    reduce_scatter x1 -> x0, waiting for transfers between devices: 44.5 us -> none  [send_back(): lax.psum_scatter(partial_out.astype(jnp.bfloat16), 'tp', scatter_dimensio...]
    psum x1 -> x0, waiting for transfers between devices: 38.7 us -> none  [local(): lax.psum(partial_attn.astype(jnp.bfloat16), 'tp').astype(jnp.float32)]
    all_gather x1 -> x0, waiting for transfers between devices: 33.3 us -> none  [local(): lax.all_gather(arrived, 'tp', axis=1, tiled=True)]
    all_to_all x1 -> x0, blocking collectives: 30.6 us -> none  [local(): lax.all_to_all(own_slots, 'sp', split_axis=0, concat_axis=0, tiled=True)]
    dot_general x6 -> x0, matrix products: 25.4 us -> none  [the longest x1 7.65 us: expert_rows(): jnp.dot(flat_rows, up_weight[0], preferred_element_type=jnp.float32)]
    all_to_all x1 -> x0, waiting for transfers between devices: 25.1 us -> none  [send_back(): return lax.all_to_all(summed, 'sp', split_axis=0, concat_axis=0, tiled=True)]
    gather x15 -> x0, local copies, waits for them, and re-layouts: 16.8 us -> none
  transfers between devices with their start and end apart: 6 -> 0, of which waited for: 4 -> 0; matrix products, arithmetic and copies ran while one was open for 4% -> 0% of each run, Pallas kernels for 0% -> 0%
where the time goes in v1:
time: 105 us
  Pallas kernels  100 us (95%)
  local copies, waits for them, and re-layouts  4.62 us (4%)
    pallas_call x1, Pallas kernels, local(): pl.pallas_call(functools.partial(layer, n, tp, cap), out_shape=jax.ShapeD...  100 us
    unnamed x3, local copies, waits for them, and re-layouts  4.62 us

profile of v1, /device:TPU:0, one launch (start us, length us, event | category | flops | bytes accessed | tf_op | source)
XLA Modules:
  0.0 105.0 jit_solution(4443241022765276440)
XLA Ops:
  0.0 1.5 %copy.13.ids_ref = s32[256,2]{1,0:T(8,128)} copy(s32[256,2]{0,1:T(2,128)} %param.19) | data formatting | bytes 4096 | tf_op args[7]
  1.5 1.5 %copy.14.rw_ref = f32[256,2]{1,0:T(8,128)} copy(f32[256,2]{0,1:T(2,128)} %param.20) | data formatting | bytes 4096 | tf_op args[8]
  3.0 100.3 %shard_map.118 = bf16[256,512]{1,0:T(8,128)(2,1)} custom-call(bf16[256,512]{1,0:T(8,128)(2,1)} %q_ref.1, bf16[256,256]{1,0:T(8,128)(2,1)} %k_ref.1, bf16[256,256]{1,0:T(8,128)(2,1)} %v_ref.1, f32[8]{0:T(128)} %sink_ref.1, f32[1,2048]{1,0:T(1,128)} %bitcast.1, s32[256,2]{1,0:T(8,128)} %copy.13.ids_ref, f32[256,2]{1,0:T(8,128)} %copy.14.rw_ref, ...), custom_call_target="tpu_custom_call" | custom-call | tf_op jit(solution)/shard_map/pallas_call | solution.py:409
  103.3 1.7 %copy.16 = bf16[256,512]{1,0:T(8,128)(2,1)} copy(bf16[256,512]{1,0:T(8,128)(2,1)} %shard_map.118) | data formatting | bytes 524288

commit v2 on v1

--- a/solution.py
+++ b/solution.py
@@ -91,6 +91,13 @@
 
     partner = at_tp(y * CORES + other)
 
+    def pair(i):
+        total, bit = 0, 1
+        while bit < n:
+            total = total + lax.rem(s // bit + i // bit, 2) * bit
+            bit *= 2
+        return total
+
     def peer_y(dy):
         return lax.rem(y + dy, ny)
 
@@ -135,15 +142,15 @@
              halo_send.at[a, 1], halo_recv.at[a, 1], left)
 
     experts = n
-    ids = ids_ref[...]
-    lanes = iota((tok, 128), 1)
-    top = ids.shape[1]
-    hits = [(lanes == ids[:, k : k + 1]).astype(F32) for k in range(top)]
+    lanes = iota((tok, 128), 1).astype(F32)
+    top = ids_ref.shape[0]
+    ids = [as_column(ids_ref[k : k + 1, :].astype(F32)) for k in range(top)]
+    hits = [(lanes == ids[k]).astype(F32) for k in range(top)]
     all_hits = functools.reduce(jnp.add, hits)
     before = (iota((tok, tok), 1) < iota((tok, tok), 0)).astype(BF16)
     earlier = dot(before, all_hits.astype(BF16))
     place = [
-        jnp.sum(earlier * hits[k], axis=1, keepdims=True) + ids[:, k : k + 1].astype(F32) * cap
+        jnp.sum(earlier * hits[k], axis=1, keepdims=True) + ids[k] * cap
         for k in range(top)
     ]
     place_row = [as_row(p) for p in place]
@@ -235,7 +242,7 @@
     xb[t, s] = rows_of(s)
 
     def dispatch(i, _):
-        e = lax.rem(s + i, n)
+        e = pair(i)
         slots[i] = rows_of(e)
         send(slots.at[i], xb.at[t, s], d_send.at[i], x_recv.at[t, s], at_sp(e))
         return 0
@@ -245,7 +252,7 @@
         load.wait()
 
     def forward(i):
-        src = lax.rem(s + n - i, n)
+        src = pair(i)
 
         @pl.when(i > 0)
         def _():
@@ -257,7 +264,7 @@
         send(xb.at[t, src], xb.at[t, src], fc_send.at[i], x_recv.at[t, src], partner)
 
     def relay(i):
-        src = lax.rem(s + n - i, n)
+        src = pair(i)
         for dy in range(1, ny):
             j = from_y(dy) * CORES + c
             landed(xb.at[j, src], x_recv.at[j, src], at_tp(j))
@@ -266,7 +273,7 @@
     tile = min(hidden, 256)
 
     def expert(i):
-        src = lax.rem(s + n - i, n)
+        src = pair(i)
         for yy in range(ny):
             j = yy * CORES + other
             landed(xb.at[j, src], x_recv.at[j, src], partner)
@@ -291,7 +298,7 @@
                  at_tp(yy * CORES + c))
 
     def finish(i):
-        src = lax.rem(s + n - i, n)
+        src = pair(i)
         total = po[i, c, y].astype(F32) + po_in[i, y].astype(F32)
         for dy in range(1, ny):
             landed(sum_y.at[dy, i], y_recv.at[dy, i], at_tp(from_y(dy) * CORES + c))
@@ -309,7 +316,7 @@
     stages = (forward, relay, expert, chip_add, finish)
 
     def step(k, _):
-        for lag, stage in enumerate(stages):
+        for lag, stage in reversed(tuple(enumerate(stages))):
             @pl.when((k >= lag) & (k - lag < n))
             def _(stage=stage, lag=lag):
                 stage(k - lag)
@@ -329,7 +336,7 @@
     mixture = jnp.zeros((tok, width), F32)
     for k in range(top):
         pick = (spot == place[k]).astype(F32).astype(BF16)
-        mixture = mixture + rw_ref[:, k : k + 1] * dot(pick, rows)
+        mixture = mixture + as_column(rw_ref[k : k + 1, :]) * dot(pick, rows)
     out_ref[...] = (residual[...].astype(F32) + mixture).astype(BF16)
 
     for a, source in enumerate((k_ref, v_ref)):
@@ -416,8 +423,8 @@
             collective_id=0, has_side_effects=True, vmem_limit_bytes=60 * 1024 * 1024
         ),
     )(
-        queries, key_columns, value_columns, sink_logits, norm_gain[None, :], expert_ids,
-        route_weights, out_weight, stream_in, gate_weight, up_weight, down_weight,
+        queries, key_columns, value_columns, sink_logits, norm_gain[None, :], expert_ids.T,
+        route_weights.T, out_weight, stream_in, gate_weight, up_weight, down_weight,
     )
 
 

time: 105 us -> 98.9 us (0.942)
  the two profiles are of different devices: /device:TPU:0 before, /device:TPU:8 now
where the time goes in v2:
time: 98.9 us; the launch traced here: 98.7 us
  Pallas kernels  97.1 us (98%)
  local copies, waits for them, and re-layouts  1.67 us (2%)
    pallas_call x1, Pallas kernels, local(): pl.pallas_call(functools.partial(layer, n, tp, cap), out_shape=jax.ShapeD...  97.1 us

profile of v2, /device:TPU:8, one launch (start us, length us, event | category | flops | bytes accessed | tf_op | source)
XLA Modules:
  0.0 98.7 jit_solution(3294008590851838673)
XLA Ops:
  0.0 97.1 %shard_map.118 = bf16[256,512]{1,0:T(8,128)(2,1)} custom-call(bf16[256,512]{1,0:T(8,128)(2,1)} %q_ref.1, bf16[256,256]{1,0:T(8,128)(2,1)} %k_ref.1, bf16[256,256]{1,0:T(8,128)(2,1)} %v_ref.1, f32[8]{0:T(128)} %sink_ref.1, f32[1,2048]{1,0:T(1,128)} %bitcast.3, s32[2,256]{1,0:T(2,128)} %bitcast.4, f32[2,256]{1,0:T(2,128)} %bitcast.5, ...), custom_call_target="tpu_custom_call" | custom-call | tf_op jit(solution)/shard_map/pallas_call | solution.py:416
  97.1 1.7 %copy.14 = bf16[256,512]{1,0:T(8,128)(2,1)} copy(bf16[256,512]{1,0:T(8,128)(2,1)} %shard_map.118) | data formatting | bytes 524288
